TPU v7x, 256 devices: a whole 4x4x8 slice. The times are simulated.
256 devices in a mesh: ep: 64 (over z, x, core), tp: 4 (over y).
Axes of the slice: x: 4, y: 4, z: 8, core: 2. Of those that a mesh axis runs over, the one named last changes fastest.
Arguments:
- queries: bfloat16 [16384, 8, 128], P('ep', 'tp'), may hold values from -256 to 256
- keys: bfloat16 [16384, 4, 128], P('ep', 'tp'), may hold values from -8 to 8
- values: bfloat16 [16384, 4, 128], P('ep', 'tp'), may hold values from -6 to 6
- attn_lambda: float32 [8], P('tp'), may hold values from 0.3 to 0.8
- head_gain: float32 [128], replicated, may hold values from 0.1 to 1.9
- w_out: bfloat16 [1024, 2048], replicated, may hold values from -0.1875 to 0.1875
- moe_rows: bfloat16 [32768, 2048], P('ep'), may hold values from -6 to 6
- moe_gain: float32 [2048], replicated, may hold values from 0.1 to 1.9
- routes: int32 [32768, 2], P('ep'), may hold values from 0 to 63, all different within a row; in each aligned block of 128 rows (0 to 127, 128 to 255, ...) at most 8 rows name the same one
- route_weights: float32 [32768, 2], P('ep'), may hold values from 0.1 to 1
- w_gate: bfloat16 [64, 2048, 1024], P('ep', None, 'tp'), may hold values from -0.125 to 0.125
- w_up: bfloat16 [64, 2048, 1024], P('ep', None, 'tp'), may hold values from -0.125 to 0.125
- w_down: bfloat16 [64, 1024, 2048], P('ep', 'tp'), may hold values from -0.1875 to 0.1875
Outputs:
- mixer_out: bfloat16 [16384, 2048], P(('ep', 'tp'))
- moe_out: bfloat16 [32768, 2048], P(('ep', 'tp'))
Inputs may be any that keep to these rules, and one draw needn't show every extreme that they name: `routes`: each row names 2 different experts. In each aligned block of 128 rows (the rows of moe_out that one device holds) no expert is named by more than 8 rows, a bound that some block reaches.
All inputs are finite; a program needn't handle non-finite values.
Results may differ from a plain program's by a relative error of at most 0.011.
Values may be sent and summed in bfloat16 or wider, within the bound.
A program may use at most 128 MiB of HBM per device.

v0:
```python
import jax
import jax.numpy as jnp
from jax import lax
from jax.sharding import PartitionSpec as P

EPSILON = 1e-06
MASKED = -1e30


def split_up(x, dim, size):
    before, after = (x.shape[:dim], x.shape[dim + 1 :])
    return jnp.moveaxis(x.reshape(*before, size, -1, *after), dim, 0)


def sum_at_owner(x, axis, dim):
    size = lax.axis_size(axis)
    tiles = lax.all_to_all(split_up(x, dim, size), axis, 0, 0, tiled=True)
    return jnp.sum(tiles.astype(jnp.float32), axis=0)


def joined_along(tiles, dim):
    tiles = jnp.moveaxis(tiles, 0, dim)
    lengths = tiles.shape
    return tiles.reshape(*lengths[:dim], lengths[dim] * lengths[dim + 1], *lengths[dim + 2 :])


def piecewise(x, axis, dim, work, out_dim):
    span = x.shape[dim]
    pieces = jnp.split(x, 2, axis=dim) if span % 2 == 0 else [x]
    first = jnp.arange(lax.axis_size(axis)) * span
    tiles = [lax.all_gather(section, axis) for section in pieces]
    made = [jax.vmap(work)(b, first + k * (span // len(pieces))) for k, b in enumerate(tiles)]
    return joined_along(jnp.concatenate(made, axis=out_dim + 1), out_dim)


def rms_scaled(values_f, gain):
    mean_sq = jnp.mean(values_f * values_f, axis=-1, keepdims=True)
    return values_f * lax.rsqrt(mean_sq + EPSILON) * gain


def slot_numbers(block_routes, experts):
    flat_ids = block_routes.reshape(-1)
    matches = (flat_ids[:, None] == lax.iota(jnp.int32, experts)[None, :]).astype(jnp.int32)
    earlier = jnp.cumsum(matches, axis=0) - matches
    return jnp.sum(earlier * matches, axis=1).reshape(block_routes.shape)


def fill_slots(block_rows, block_routes, experts, capacity):
    slot_ids = slot_numbers(block_routes, experts)
    model_width = block_rows.shape[1]
    copies = jnp.broadcast_to(block_rows[:, None, :], block_routes.shape + (model_width,))
    blank_slots = jnp.zeros((experts, capacity, model_width), block_rows.dtype)
    return (blank_slots.at[block_routes, slot_ids].set(copies), slot_ids)


def local(
    queries,
    keys,
    values,
    attn_lambda,
    head_gain,
    w_out,
    moe_rows,
    moe_gain,
    routes,
    route_weights,
    w_gate,
    w_up,
    w_down,
):
    positions = queries.shape[0]
    q_heads = queries.shape[1]
    kv_heads = keys.shape[1]
    head_dim = queries.shape[2] // 2
    value_dim = values.shape[2]
    per_key = q_heads // kv_heads
    first_pos = lax.axis_index("ep") * positions
    query_pos = first_pos + lax.iota(jnp.int32, positions)
    last_pos = first_pos + positions - 1
    query_view = queries.reshape(positions, kv_heads, per_key, 2, head_dim)
    inv_scale = head_dim ** (-0.5)
    start_max = jnp.full((positions, kv_heads, per_key, 2), MASKED, jnp.float32)
    start_total = jnp.zeros((positions, kv_heads, per_key, 2), jnp.float32)
    start_acc = jnp.zeros((positions, kv_heads, per_key, 2, value_dim), jnp.float32)
    carry = (start_max, start_total, start_acc)
    key_piece = lax.all_gather(keys, "ep", axis=0, tiled=True)
    value_piece = lax.all_gather(values, "ep", axis=0, tiled=True)
    shard_count = key_piece.shape[0] // positions
    together = 1
    for candidate in (2, 3, 4):
        if shard_count % candidate == 0:
            together = candidate
    block_len = together * positions
    blocks = shard_count // together
    key_blocks = key_piece.reshape(blocks, block_len, kv_heads, 2, head_dim)
    value_blocks = value_piece.reshape(blocks, block_len, kv_heads, value_dim)
    block_starts = block_len * lax.iota(jnp.int32, blocks)

    def visit(running, inputs):
        key_blk, value_blk, block_start = inputs

        def update(current):
            run_max, run_total, run_acc = current
            key_pos = block_start + lax.iota(jnp.int32, block_len)
            scores = (
                jnp.einsum(
                    "qkgmd,pkmd->qkgmp", query_view, key_blk, preferred_element_type=jnp.float32
                )
                * inv_scale
            )
            allowed = key_pos[None, :] <= query_pos[:, None]
            scores = jnp.where(allowed[:, None, None, None, :], scores, MASKED)
            new_max = jnp.maximum(run_max, jnp.max(scores, axis=-1))
            shrink = jnp.exp(run_max - new_max)
            weights = jnp.exp(scores - new_max[..., None])
            run_total = run_total * shrink + jnp.sum(weights, axis=-1)
            run_acc = run_acc * shrink[..., None] + jnp.einsum(
                "qkgmp,pkv->qkgmv",
                weights.astype(jnp.bfloat16),
                value_blk,
                preferred_element_type=jnp.float32,
            )
            return (new_max, run_total, run_acc)

        def keep(current):
            return current

        return (lax.cond(block_start <= last_pos, update, keep, running), None)

    carry, unused = lax.scan(visit, carry, (key_blocks, value_blocks, block_starts))
    run_max, run_total, run_acc = carry
    ratios = run_acc / run_total[..., None]
    lambda_view = attn_lambda.reshape(1, kv_heads, per_key, 1)
    head_out = ratios[:, :, :, 0] - lambda_view * ratios[:, :, :, 1]
    attn_rows = (
        rms_scaled(head_out, head_gain).astype(jnp.bfloat16).reshape(positions, q_heads * value_dim)
    )
    tp_count = lax.axis_size("tp")
    tp_id = lax.axis_index("tp")
    head_width = q_heads * value_dim
    w_local = lax.dynamic_slice_in_dim(w_out, tp_id * head_width, head_width, 0)
    mixer_out = sum_at_owner(
        jnp.dot(attn_rows, w_local, preferred_element_type=jnp.float32).astype(jnp.bfloat16),
        "tp",
        0,
    ).astype(jnp.bfloat16)
    experts = lax.axis_size("ep")
    dev_rows = moe_rows.shape[0] // tp_count
    top_count = routes.shape[1]
    capacity = max(2, 2 * dev_rows * top_count // experts)
    model_width = moe_rows.shape[1]
    hidden_units = w_gate.shape[2]
    own_routes = lax.dynamic_slice_in_dim(routes, tp_id * dev_rows, dev_rows, 0)
    own_weights = lax.dynamic_slice_in_dim(route_weights, tp_id * dev_rows, dev_rows, 0)

    def expert_hidden(slot_rows):
        flat_rows = slot_rows.reshape(-1, model_width)
        gate_out = jnp.dot(flat_rows, w_gate[0], preferred_element_type=jnp.float32)
        up_out = jnp.dot(flat_rows, w_up[0], preferred_element_type=jnp.float32)
        return (
            (jax.nn.silu(gate_out) * up_out)
            .astype(jnp.bfloat16)
            .reshape(slot_rows.shape[:-1] + (hidden_units,))
        )

    own_rows = rms_scaled(
        lax.dynamic_slice_in_dim(moe_rows, tp_id * dev_rows, dev_rows, 0).astype(jnp.float32),
        moe_gain,
    ).astype(jnp.bfloat16)
    outgoing, own_slots = fill_slots(own_rows, own_routes, experts, capacity)
    arrived = lax.all_to_all(outgoing, "ep", split_axis=0, concat_axis=0, tiled=True)

    def hidden_piece(slot_rows, begin_row):
        return expert_hidden(slot_rows)

    hidden = piecewise(arrived[None], "tp", 0, hidden_piece, 0)
    all_units = lax.all_to_all(hidden, "tp", split_axis=0, concat_axis=3, tiled=True)
    down_whole = lax.all_gather(w_down[0], "tp", axis=0, tiled=True)
    flat_units = all_units.reshape(-1, tp_count * hidden_units)
    summed_f = jnp.zeros((flat_units.shape[0], model_width), jnp.float32)
    for group in range(tp_count):
        unit_block = flat_units[:, group * hidden_units : (group + 1) * hidden_units]
        weight_block = down_whole[group * hidden_units : (group + 1) * hidden_units]
        group_part = jnp.dot(unit_block, weight_block, preferred_element_type=jnp.float32).astype(
            jnp.bfloat16
        )
        summed_f = summed_f + group_part.astype(jnp.float32)
    summed = summed_f.astype(jnp.bfloat16).reshape(all_units.shape[:-1] + (model_width,))
    returned = lax.all_to_all(summed, "ep", split_axis=1, concat_axis=1, tiled=True)[0]
    picked = returned[own_routes, own_slots]
    moe_out = jnp.sum(own_weights[..., None] * picked.astype(jnp.float32), axis=1).astype(
        jnp.bfloat16
    )
    return (mixer_out, moe_out)


def solution(mesh):
    return jax.shard_map(
        local,
        mesh=mesh,
        in_specs=(
            P("ep", "tp", None),
            P("ep", "tp", None),
            P("ep", "tp", None),
            P("tp"),
            P(),
            P(),
            P("ep", None),
            P(),
            P("ep", None),
            P("ep", None),
            P("ep", None, "tp"),
            P("ep", None, "tp"),
            P("ep", "tp", None),
        ),
        out_specs=(P(("ep", "tp"), None), P(("ep", "tp"), None)),
        check_vma=False,
    )
```

profile of v0, /device:TPU:7, one launch (start us, length us, event | category | flops | bytes accessed | tf_op | source)
XLA Modules:
  0.0 432.9 jit_solution(10305571413842020620)
XLA Ops:
  7.2 0.7 all-gather.7.cloned.1.call-update
  8.0 0.7 all-gather.9.cloned.1.call-update
  8.7 0.7 constant_dynamic-slice_fusion
  9.8 0.6 reduce-window.6
  11.1 1.2 fusion.25
  12.3 1.3 fusion.27
  13.6 0.6 broadcast_in_dim.57
  14.2 1.2 reshape.247
  15.7 33.0 %scatter_fusion = bf16[64,8,2048]{2,1,0:T(8,128)(2,1)S(1)} fusion(bf16[64,8,2048]{2,1,0:T(8,128)(2,1)S(1)} %broadcast_in_dim.36, s32[256]{0:T(256)S(1)} %reshape.245, bf16[256,2048]{1,0:T(8,128)(2,1)} %reshape.247), kind=kCustom, calls=%fused_computation.1 | custom fusion | bytes 3147776 | tf_op jit(solution)/shard_map/scatter | solution.py:53
  48.8 71.2 %all_to_all.30 = bf16[64,8,2048]{2,1,0:T(8,128)(2,1)} all-to-all(bf16[64,8,2048]{2,1,0:T(8,128)(2,1)S(1)} %scatter_fusion), channel_id=1, replica_groups=mesh['ep'=64,'tp'=4] {'ep'}, dimensions={0} | all-to-all | bytes 4194304 | tf_op jit(solution)/shard_map/all_to_all | solution.py:171
  120.8 14.7 %reshape.263 = bf16[16,1024,1,2,64]{4,3,1,0,2:T(2,128)(2,1)} reshape(bf16[16384,1,128]{2,0,1:T(8,128)(2,1)} %all-gather.7.cloned.1.call-done) | data formatting | bytes 8388608 | tf_op jit(solution)/shard_map/reshape | solution.py:95
  135.5 20.2 %copy.37 = bf16[16,1024,1,2,64]{1,4,3,2,0:T(8,128)(2,1)} copy(bf16[16,1024,1,2,64]{4,3,1,0,2:T(2,128)(2,1)} %reshape.263) | data formatting | bytes 8388608
  155.7 31.6 %all-gather.9.cloned.1.call-done = bf16[16384,1,128]{2,0,1:T(8,128)(2,1)} async-done(((bf16[256,1,128]{2,0,1:T(8,128)(2,1)}), bf16[16384,1,128]{2,0,1:T(8,128)(2,1)}) %all-gather.9.cloned.1.call-update) | async-done | bytes 4194320 | tf_op jit(solution)/shard_map/all_gather | solution.py:87
  187.3 6.4 %copy.39 = bf16[16,1024,1,128]{1,3,2,0:T(8,128)(2,1)} copy(bf16[16,1024,1,128]{3,1,0,2:T(8,128)(2,1)} %bitcast.160) | data formatting | bytes 8388608
  193.7 29.0 %while.15 = (s32[]{:T(128)}, f32[256,1,2,2]{0,2,3,1:T(2,128)S(1)}, f32[256,1,2,2]{0,2,3,1:T(2,128)S(1)}, f32[256,1,2,2,128]{0,4,3,2,1:T(8,128)S(1)}, s32[16]{0:T...) while((s32[]{:T(128)}, f32[256,1,2,2]{0,2,3,1:T(2,128)S(1)}, ...), condition=%wide.region_5.6_spmd.clone, body=%wide.region_0.5_spmd.clone.sunk | while | flops 411570432 | bytes 15156511 | solution.py:130
  193.7 0.6 dynamic_slice.56
  194.8 5.2 %conditional.3 = ((f32[256,1,2,2]{0,2,3,1:T(2,128)S(1)}, f32[256,1,2,2]{0,2,3,1:T(2,128)S(1)}, f32[256,1,2,2,128]{0,4,3,2,1:T(8,128)S(1)})) conditional(s32[]{:T(128)} %convert_element_type.131, (f32[256,1,2,2]{0,2,3,1:T(2,128)S(1)}, f32[256,1,2,2]{0,2,3,1:T(2,128)S(1)}, f32[256,1,2,2,128]{0,4,3,2,1:T(8,128)S(1)}) %tuple.48, (s32[]{:T(128)}, ...), branch_computations={%region_1.1_spmd, %region_2.4_spmd} | conditional | flops 411570432 | bytes 15155240 | solution.py:128
  195.6 1.8 fusion.4
  197.5 1.0 fusion.5
  198.5 1.5 fusion.11
  200.1 0.6 dynamic_slice.56
  201.2 5.2 %conditional.3 = ((f32[256,1,2,2]{0,2,3,1:T(2,128)S(1)}, f32[256,1,2,2]{0,2,3,1:T(2,128)S(1)}, f32[256,1,2,2,128]{0,4,3,2,1:T(8,128)S(1)})) conditional(s32[]{:T(128)} %convert_element_type.131, (f32[256,1,2,2]{0,2,3,1:T(2,128)S(1)}, f32[256,1,2,2]{0,2,3,1:T(2,128)S(1)}, f32[256,1,2,2,128]{0,4,3,2,1:T(8,128)S(1)}) %tuple.48, (s32[]{:T(128)}, ...), branch_computations={%region_1.1_spmd, %region_2.4_spmd} | conditional | flops 411570432 | bytes 15155240 | solution.py:128
  202.0 1.8 fusion.4
  203.9 1.0 fusion.5
  204.9 1.5 fusion.11
  207.6 0.6 dynamic_slice.56
  208.8 0.6 dynamic_slice.56
  222.8 50.1 %all-gather.11.cloned.1.call-done = bf16[256,8,2048]{2,1,0:T(8,128)(2,1)} async-done(((bf16[64,8,2048]{2,1,0:T(8,128)(2,1)}), bf16[256,8,2048]{2,1,0:T(8,128)(2,1)}) %all-gather.11.cloned.1.call-update) | async-done | bytes 8388624 | tf_op jit(solution)/shard_map/all_gather | solution.py:31
  272.9 5.9 %fusion.28 = f32[4,512,256]{2,1,0:T(8,128)S(1)} fusion(bf16[4,512,2048]{2,1,0:T(8,128)(2,1)} %bitcast.170, bf16[1,2048,256]{2,1,0:T(8,128)(2,1)S(1)} %copy-done), kind=kOutput, calls=%fused_computation.47 | convolution fusion | flops 2147483648 | bytes 11534336 | tf_op jit(solution)/shard_map/vmap()/dot_general | solution.py:159
  278.9 3.6 fusion.24
  282.5 3.7 all-to-all-start.2
  286.5 2.8 convolution_convert_fusion.4
  289.3 18.2 %all-to-all-done.2 = bf16[4,64,8,256]{3,2,1,0:T(8,128)(2,1)S(1)} async-done(((bf16[4,64,8,256]{3,2,1,0:T(8,128)(2,1)}), bf16[4,64,8,256]{3,2,1,0:T(8,128)(2,1)S(1)}, u32[]{:S(2)}, u32[]{:S(2)}) %all-to-all-start.2) | async-done | bytes 1048608 | tf_op jit(solution)/shard_map/all_to_all | solution.py:177
  307.4 3.7 all-to-all-start
  311.2 1.4 copy.65
  312.8 33.9 %all-gather.13.cloned.1.call-done = bf16[1,1024,2048]{2,1,0:T(8,128)(2,1)} async-done(((bf16[1,256,2048]{2,1,0:T(8,128)(2,1)}), bf16[1,1024,2048]{2,1,0:T(8,128)(2,1)}) %all-gather.13.cloned.1.call-update) | async-done | bytes 4194320 | tf_op jit(solution)/shard_map/all_gather | solution.py:178
  346.7 2.1 convolution_convert_fusion
  348.8 1.9 convolution_convert_fusion.1
  350.7 0.7 convolution_convert_fusion.2
  351.5 2.6 fusion.23
  354.1 1.0 copy-done.2
  355.0 10.7 %all-to-all-start.3 = ((bf16[1,64,8,2048]{3,2,0,1:T(8,128)(2,1)}), bf16[1,64,8,2048]{3,2,0,1:T(8,128)(2,1)S(1)}, u32[]{:S(2)}, u32[]{:S(2)}) async-start(bf16[1,64,8,2048]{3,2,0,1:T(8,128)(2,1)} %fusion.23), calls=%async_computation.3 | async-start | bytes 4194304 | tf_op jit(solution)/shard_map/all_to_all | solution.py:189
  365.9 0.7 constant_dynamic-slice_fusion.1
  366.7 2.2 reduce_sum.60
  368.9 46.0 %all-to-all-done.3 = bf16[1,64,8,2048]{3,2,0,1:T(8,128)(2,1)S(1)} async-done(((bf16[1,64,8,2048]{3,2,0,1:T(8,128)(2,1)}), bf16[1,64,8,2048]{3,2,0,1:T(8,128)(2,1)S(1)}, u32[]{:S(2)}, u32[]{:S(2)}) %all-to-all-start.3) | async-done | bytes 2097184 | tf_op jit(solution)/shard_map/all_to_all | solution.py:189
  414.8 5.2 %gather_fusion = bf16[256,2048]{1,0:T(8,128)(2,1)} fusion(bf16[64,8,2048]{2,1,0:T(8,128)(2,1)S(1)} %bitcast.159, s32[256]{0:T(256)S(1)} %reshape.239), kind=kCustom, calls=%fused_computation | custom fusion | bytes 2099200 | tf_op jit(solution)/shard_map/gather | solution.py:190
  420.1 2.4 reshape.258
  422.4 3.9 multiply_reduce_fusion
  (108 shorter events, 11.8 us)
Async XLA Ops:
  7.2 265.7 %copy-start = (bf16[1,2048,256]{2,1,0:T(8,128)(2,1)S(1)}, bf16[1,2048,256]{2,1,0:T(8,128)(2,1)}, u32[]{:S(2)}) copy-start(bf16[1,2048,256]{2,1,0:T(8,128)(2,1)} %param.28) | copy-start | bytes 3145732
  7.2 113.6 %all-gather.7.cloned.1.call-start = ((), (), s32[]{:S(2)}) async-start(), calls=%async_computation.4 | async-start | bytes 4259840 | tf_op jit(solution)/shard_map/all_gather | solution.py:86
  7.9 179.4 %all-gather.9.cloned.1.call-start = ((), (), s32[]{:S(2)}) async-start(), calls=%async_computation.5 | async-start | bytes 4259840 | tf_op jit(solution)/shard_map/all_gather | solution.py:87
  8.7 264.2 %all-gather.11.cloned.1.call-start = ((), (), s32[]{:S(2)}) async-start(), calls=%async_computation.6 | async-start | bytes 10485760 | tf_op jit(solution)/shard_map/all_gather | solution.py:31
  48.7 71.9 %copy-start.3 = (bf16[256,2,128]{2,1,0:T(2,128)(2,1)S(1)}, bf16[256,2,128]{2,1,0:T(2,128)(2,1)}, u32[]{:S(2)}) copy-start(bf16[256,2,128]{2,1,0:T(2,128)(2,1)} %param.17) | copy-start | bytes 393220
  48.7 72.0 %copy-start.4 = (f32[2]{0:T(128)S(1)}, f32[2]{0:T(128)}, u32[]{:S(2)}) copy-start(f32[2]{0:T(128)} %param.20) | copy-start | bytes 28
  48.7 72.0 %copy-start.5 = (f32[128]{0:T(128)S(1)}, f32[128]{0:T(128)}, u32[]{:S(2)}) copy-start(f32[128]{0:T(128)} %param.21) | copy-start | bytes 1540
  120.0 226.7 %all-gather.13.cloned.1.call-start = ((), (), s32[]{:S(2)}) async-start(), calls=%async_computation.7 | async-start | bytes 5242880 | tf_op jit(solution)/shard_map/all_gather | solution.py:178
  272.9 5.9 %copy-start.6 = (bf16[256,8,2048]{2,1,0:T(8,128)(2,1)S(1)}, bf16[256,8,2048]{2,1,0:T(8,128)(2,1)}, u32[]{:S(2)}) copy-start(bf16[256,8,2048]{2,1,0:T(8,128)(2,1)} %all-gather.11.cloned.1.call-done) | copy-start | bytes 25165828
  272.9 6.0 %copy-start.7 = (bf16[1,2048,256]{2,1,0:T(8,128)(2,1)S(1)}, bf16[1,2048,256]{2,1,0:T(8,128)(2,1)}, u32[]{:S(2)}) copy-start(bf16[1,2048,256]{2,1,0:T(8,128)(2,1)} %param.27) | copy-start | bytes 3145732
  282.5 24.9 %all-to-all-start.2 = ((bf16[4,64,8,256]{3,2,1,0:T(8,128)(2,1)}), bf16[4,64,8,256]{3,2,1,0:T(8,128)(2,1)S(1)}, u32[]{:S(2)}, u32[]{:S(2)}) async-start(bf16[4,64,8,256]{3,2,1,0:T(8,128)(2,1)} %fusion.24), calls=%async_computation.2 | async-start | bytes 2097152 | tf_op jit(solution)/shard_map/all_to_all | solution.py:177
  307.4 46.6 %all-to-all-start = ((bf16[4,64,2048]{2,1,0:T(8,128)(2,1)}), bf16[4,64,2048]{2,1,0:T(8,128)(2,1)S(1)}, u32[]{:S(2)}, u32[]{:S(2)}) async-start(bf16[4,64,2048]{2,1,0:T(8,128)(2,1)} %bitcast.26), calls=%async_computation | async-start | bytes 2097152 | tf_op jit(solution)/shard_map/all_to_all | solution.py:17
  346.7 4.0 copy-start.1
  354.1 1.0 copy-start.2
  355.0 59.8 %all-to-all-start.3 = ((bf16[1,64,8,2048]{3,2,0,1:T(8,128)(2,1)}), bf16[1,64,8,2048]{3,2,0,1:T(8,128)(2,1)S(1)}, u32[]{:S(2)}, u32[]{:S(2)}) async-start(bf16[1,64,8,2048]{3,2,0,1:T(8,128)(2,1)} %fusion.23), calls=%async_computation.3 | async-start | bytes 4194304 | tf_op jit(solution)/shard_map/all_to_all | solution.py:189
Sparse Core Ops, SparseCore 0:
  10.8 92.8 all-gather.6
  106.4 80.7 all-gather.8
  189.1 83.7 all-gather.10
  274.6 72.0 all-gather.12
where the time goes:
time: 438 us; the launch traced here: 433 us
  waiting for transfers between devices  181 us (41%)
  local copies, waits for them, and re-layouts  98.3 us (22%)
  blocking collectives  71.2 us (16%)
  matrix products  26.3 us (6%)
  starting transfers between devices  18.4 us (4%)
  between operations  14.1 us (3%)
  other arithmetic  13.3 us (3%)
  loops' own time  9.78 us (2%)
    all_to_all x1, blocking collectives, local(): lax.all_to_all(outgoing, 'ep', split_axis=0, concat_axis=0, tiled=True)  71.2 us
    all_gather x1, waiting for transfers between devices, piecewise(): tiles = [lax.all_gather(section, axis) for section in pieces]  50.1 us
    all_to_all x1, waiting for transfers between devices, local(): lax.all_to_all(summed, 'ep', split_axis=1, concat_axis=1, tiled=True)[0]  46 us
    all_gather x1, waiting for transfers between devices, local(): down_whole = lax.all_gather(w_down[0], 'tp', axis=0, tiled=True)  33.9 us
    scatter x1, local copies, waits for them, and re-layouts, fill_slots(): return (blank_slots.at[block_routes, slot_ids].set(copies), slot_ids)  33 us
    all_gather x1, waiting for transfers between devices, local(): value_piece = lax.all_gather(values, 'ep', axis=0, tiled=True)  31.6 us
    unnamed x22, local copies, waits for them, and re-layouts  28.1 us
    all_to_all x1, waiting for transfers between devices, local(): lax.all_to_all(hidden, 'tp', split_axis=0, concat_axis=3, tiled=True)  18.2 us
  transfers between devices with their start and end apart: 7, of which 5 were waited for; matrix products, arithmetic and copies ran while one was open for 29% of the time, Pallas kernels for 0%

commit v1 on v0

v1 whole, which is shorter than its diff:
```python
import functools

import jax
import jax.numpy as jnp
from jax import lax
from jax.experimental import pallas as pl
from jax.experimental.pallas import tpu as pltpu
from jax.sharding import PartitionSpec as P

EPSILON = 1e-06
MASKED = -1e30
MESH = pl.DeviceIdType.MESH
CAP = 8
BF = jnp.bfloat16
F32 = jnp.float32
ANY = pl.BlockSpec(memory_space=pl.ANY)
VM = pl.BlockSpec(memory_space=pltpu.VMEM)


def one_hot_slots(route_a, route_b, shape, token_dim, counts):
    slot_dim = 1 - token_dim
    slot = lax.broadcasted_iota(jnp.int32, shape, slot_dim)
    expert = slot // CAP
    place = (slot - expert * CAP).astype(F32)
    hit_a, hit_b = route_a == expert, route_b == expert
    hit = (hit_a | hit_b).astype(F32).astype(BF)
    earlier = counts(hit)
    here = earlier == place
    return hit_a & here, hit_b & here


def pack_kernel(rows_ref, gain_ref, routes_ref, out_ref):
    tokens = rows_ref.shape[0]
    slots = out_ref.shape[0]
    rows = rows_ref[...].astype(F32)
    mean_sq = jnp.mean(rows * rows, axis=-1, keepdims=True)
    normed = (rows * lax.rsqrt(mean_sq + EPSILON) * gain_ref[...]).astype(BF)
    before = (
        lax.broadcasted_iota(jnp.int32, (tokens, tokens), 0)
        < lax.broadcasted_iota(jnp.int32, (tokens, tokens), 1)
    )
    before = before.astype(F32).astype(BF)

    def counts(hit):
        return jnp.dot(hit, before, preferred_element_type=F32)

    first, second = one_hot_slots(
        routes_ref[0:1, :], routes_ref[1:2, :], (slots, tokens), 1, counts
    )
    pick = (first | second).astype(F32).astype(BF)
    step = 256
    for n in range(0, rows_ref.shape[1], step):
        out_ref[:, n : n + step] = jnp.dot(
            pick, normed[:, n : n + step], preferred_element_type=F32
        ).astype(BF)


def combine_kernel(back_ref, routes_ref, weights_ref, out_ref):
    tokens = out_ref.shape[0]
    slots = back_ref.shape[0]
    before = (
        lax.broadcasted_iota(jnp.int32, (tokens, tokens), 1)
        < lax.broadcasted_iota(jnp.int32, (tokens, tokens), 0)
    )
    before = before.astype(F32).astype(BF)

    def counts(hit):
        return jnp.dot(before, hit, preferred_element_type=F32)

    first, second = one_hot_slots(
        routes_ref[:, 0:1], routes_ref[:, 1:2], (tokens, slots), 0, counts
    )
    mix = jnp.where(first, weights_ref[:, 0:1], 0.0) + jnp.where(second, weights_ref[:, 1:2], 0.0)
    high = mix.astype(BF)
    low = (mix - high.astype(F32)).astype(BF)
    step = 256
    for n in range(0, out_ref.shape[1], step):
        part = back_ref[:, n : n + step]
        out_ref[:, n : n + step] = (
            jnp.dot(high, part, preferred_element_type=F32)
            + jnp.dot(low, part, preferred_element_type=F32)
        ).astype(BF)


def comm_kernel(
    n_ep, n_tp, nz, nx,
    slots_ref, kv_ref, wg_ref, wu_ref, wd_ref,
    arrived_ref, kv_all_ref, g_ref, u_ref, d_ref,
    slot_tmp, kv_tmp, w_tmp, wd_tmp,
    w_send, w_recv, f_send, f_recv, z_send, z_recv, x_send, x_recv, y_send, y_recv,
    c_send, c_recv, d_send, d_recv, local_sem,
):
    me = lax.axis_index("ep")
    tp = lax.axis_index("tp")
    z = me // (2 * nx)
    x = (me // 2) % nx
    c = me % 2

    def ep_of(zz, xx, cc):
        return zz * (2 * nx) + xx * 2 + cc

    barrier = pltpu.get_barrier_semaphore()

    def greet(d, carry):
        pl.semaphore_signal(
            barrier, inc=1, device_id={"ep": lax.rem(me + d, n_ep)}, device_id_type=MESH
        )
        return carry

    lax.fori_loop(1, n_ep, greet, 0)
    for d in range(1, n_tp):
        pl.semaphore_signal(
            barrier, inc=1, device_id={"tp": lax.rem(tp + d, n_tp)}, device_id_type=MESH
        )
    pl.semaphore_wait(barrier, n_ep - 1 + n_tp - 1)

    def remote(src, dst, send, recv, where):
        return pltpu.make_async_remote_copy(
            src_ref=src, dst_ref=dst, send_sem=send, recv_sem=recv,
            device_id=where, device_id_type=MESH,
        )

    up, down = {"tp": lax.rem(tp + 1, n_tp)}, {"tp": lax.rem(tp + n_tp - 1, n_tp)}
    pairs = ((wg_ref, g_ref), (wu_ref, u_ref), (wd_ref, d_ref))

    def z_copy(k):
        to = ep_of(lax.rem(z + k, nz), x, c)
        return remote(kv_ref, kv_all_ref.at[z, x, c], z_send.at[k], z_recv.at[k], {"ep": to})

    for k in range(1, nz):
        z_copy(k).start()
    weights = []
    for i, (src, dst) in enumerate(pairs):
        for s, where in enumerate((up, down)):
            w = remote(src, dst.at[tp], w_send.at[s, i], w_recv.at[s, i], where)
            w.start()
            weights.append(w)

    def row_copy(d):
        to = lax.rem(me + d, n_ep)
        return remote(
            slots_ref.at[to], arrived_ref.at[me], d_send.at[d], d_recv.at[d], {"ep": to}
        )

    def row_start(d, carry):
        row_copy(d).start()
        return carry

    half = n_ep // 2
    lax.fori_loop(1, half, row_start, 0)

    def stay(src, tmp, dst, n):
        pull = pltpu.make_async_copy(src, tmp, local_sem.at[n])
        pull.start()
        pull.wait()
        push = pltpu.make_async_copy(tmp, dst, local_sem.at[n])
        push.start()
        push.wait()

    stay(kv_ref, kv_tmp, kv_all_ref.at[z, x, c], 0)
    stay(slots_ref.at[me], slot_tmp, arrived_ref.at[me], 1)
    stay(wg_ref, w_tmp, g_ref.at[tp], 2)
    stay(wu_ref, w_tmp, u_ref.at[tp], 2)
    stay(wd_ref, wd_tmp, d_ref.at[tp], 3)

    for k in range(1, nz):
        z_copy(k).wait()

    xr, xl = lax.rem(x + 1, nx), lax.rem(x + nx - 1, nx)
    x2 = lax.rem(x + 2, nx)
    right, left = {"ep": ep_of(z, xr, c)}, {"ep": ep_of(z, xl, c)}
    twin = {"ep": ep_of(z, x, 1 - c)}

    def column(xx):
        return kv_all_ref.at[:, xx, c]

    def across(n, xx):
        return remote(column(xx), column(xx), c_send.at[n], c_recv.at[n], twin)

    to_right = remote(column(x), column(x), x_send.at[0], x_recv.at[0], right)
    to_left = remote(column(x), column(x), x_send.at[1], x_recv.at[1], left)
    to_right.start()
    to_left.start()
    across(0, x).start()
    lax.fori_loop(half, n_ep, row_start, 0)

    def forward(i):
        src, dst = pairs[i]
        mid = src.shape[0] // 2
        came_up, came_down = lax.rem(tp + n_tp - 1, n_tp), lax.rem(tp + 1, n_tp)
        low, high = pl.ds(0, mid), pl.ds(mid, mid)
        return (
            remote(dst.at[came_up, low], dst.at[came_up, low], f_send.at[0, i], f_recv.at[0, i], up),
            remote(
                dst.at[came_down, high], dst.at[came_down, high], f_send.at[1, i], f_recv.at[1, i], down
            ),
        )

    def pass_on(i):
        for w in weights[2 * i : 2 * i + 2]:
            w.wait_recv()
        for f in forward(i):
            f.start()

    pass_on(0)
    pass_on(1)

    to_right.wait_recv()
    hz = nz // 2
    on_right = remote(
        kv_all_ref.at[pl.ds(0, hz), xl, c], kv_all_ref.at[pl.ds(0, hz), xl, c],
        y_send.at[0], y_recv.at[0], right,
    )
    on_right.start()
    across(1, xl).start()
    to_left.wait_recv()
    on_left = remote(
        kv_all_ref.at[pl.ds(hz, hz), xr, c], kv_all_ref.at[pl.ds(hz, hz), xr, c],
        y_send.at[1], y_recv.at[1], left,
    )
    on_left.start()
    across(2, xr).start()
    pass_on(2)
    on_right.wait_recv()
    on_left.wait_recv()
    across(3, x2).start()

    def row_wait(d, carry):
        row_copy(d).wait()
        return carry

    lax.fori_loop(1, n_ep, row_wait, 0)
    for n, xx in enumerate((x, xl, xr, x2)):
        across(n, xx).wait()
    for w in weights:
        w.wait_send()
    for i in range(3):
        for f in forward(i):
            f.wait()
    for w in (to_right, to_left, on_right, on_left):
        w.wait_send()


def expert_kernel(rows_ref, g_ref, u_ref, d_ref, out_ref, acc_ref):
    g = pl.program_id(0)

    @pl.when(g == 0)
    def _():
        acc_ref[...] = jnp.zeros_like(acc_ref)

    step = 256
    for m in range(0, rows_ref.shape[0], step):
        rows = rows_ref[m : m + step, :]
        gate = jnp.dot(rows, g_ref[0], preferred_element_type=F32)
        upper = jnp.dot(rows, u_ref[0], preferred_element_type=F32)
        hidden = (gate / (1.0 + jnp.exp(-gate)) * upper).astype(BF)
        for n in range(0, out_ref.shape[1], 512):
            part = jnp.dot(hidden, d_ref[0, :, n : n + 512], preferred_element_type=F32)
            acc_ref[m : m + step, n : n + 512] += part.astype(BF).astype(F32)

    @pl.when(g == pl.num_programs(0) - 1)
    def _():
        out_ref[...] = acc_ref[...].astype(BF)


def attention_kernel(blk, q_ref, kv_ref, lam_ref, gain_ref, out_ref, q_s, m_s, acc_s):
    me = lax.axis_index("ep")
    rows = q_ref.shape[1]
    heads = q_ref.shape[0]
    vdim = q_ref.shape[2]
    hd = vdim // 2
    lane = lax.broadcasted_iota(jnp.int32, (rows, vdim), 1)
    for h in range(heads):
        q = q_ref[h] * jnp.asarray(hd**-0.5, BF)
        for m in range(2):
            q_s[2 * h + m] = jnp.where((lane // hd) == m, q, jnp.zeros_like(q))
    m_s[...] = jnp.full_like(m_s, MASKED)
    acc_s[...] = jnp.zeros_like(acc_s)

    def block(b, masked):
        start = pl.multiple_of(b * blk, blk)
        k = kv_ref[pl.ds(start, blk), 0:vdim]
        v = kv_ref[pl.ds(start, blk), vdim : 2 * vdim]
        v_one = jnp.concatenate([v, jnp.ones_like(v)], axis=1)
        for r in range(2 * heads):
            s = lax.dot_general(
                q_s[r], k, (((1,), (1,)), ((), ())), preferred_element_type=F32
            )
            if masked:
                kp = start + lax.broadcasted_iota(jnp.int32, s.shape, 1)
                qp = me * rows + lax.broadcasted_iota(jnp.int32, s.shape, 0)
                s = jnp.where(kp <= qp, s, MASKED)
            old = m_s[r]
            new = jnp.maximum(old, jnp.max(s, axis=1, keepdims=True))
            shrink = jnp.exp(old - new)
            p = jnp.exp(s - new[:, 0:1]).astype(BF)
            m_s[r] = new
            acc_s[r] = acc_s[r] * shrink[:, 0:1] + jnp.dot(p, v_one, preferred_element_type=F32)

    last = (me * rows) // blk

    def body(b, carry):
        block(b, False)
        return carry

    lax.fori_loop(0, last, body, 0)
    block(last, True)
    for h in range(heads):
        ratio = [acc_s[2 * h + m][:, 0:vdim] / acc_s[2 * h + m][:, vdim:] for m in range(2)]
        out = ratio[0] - lam_ref[h] * ratio[1]
        mean_sq = jnp.mean(out * out, axis=-1, keepdims=True)
        out_ref[:, h * vdim : (h + 1) * vdim] = (
            out * lax.rsqrt(mean_sq + EPSILON) * gain_ref[...]
        ).astype(BF)


def params(**kw):
    return pltpu.CompilerParams(vmem_limit_bytes=48 * 1024 * 1024, **kw)


def local(
    queries, keys, values, attn_lambda, head_gain, w_out,
    moe_rows, moe_gain, routes, route_weights, w_gate, w_up, w_down,
):
    n_ep, n_tp = lax.axis_size("ep"), lax.axis_size("tp")
    nx = 4
    nz = n_ep // (2 * nx)
    tp = lax.axis_index("tp")
    positions, heads, vdim = queries.shape
    width = moe_rows.shape[1]
    dev_rows = moe_rows.shape[0] // n_tp
    slots = n_ep * CAP
    hid = w_gate.shape[2]

    own_rows = lax.dynamic_slice_in_dim(moe_rows, tp * dev_rows, dev_rows, 0)
    own_routes = lax.dynamic_slice_in_dim(routes, tp * dev_rows, dev_rows, 0)
    own_weights = lax.dynamic_slice_in_dim(route_weights, tp * dev_rows, dev_rows, 0)

    outgoing = pl.pallas_call(
        pack_kernel,
        out_shape=jax.ShapeDtypeStruct((slots, width), BF),
        in_specs=[VM, VM, VM],
        out_specs=VM,
        compiler_params=params(),
        name="pack",
    )(own_rows, moe_gain.reshape(1, width), own_routes.T)

    kv = jnp.concatenate([keys[:, 0], values[:, 0]], axis=1)
    sem = pltpu.SemaphoreType.DMA
    arrived, kv_all, g_all, u_all, d_all = pl.pallas_call(
        functools.partial(comm_kernel, n_ep, n_tp, nz, nx),
        out_shape=[
            jax.ShapeDtypeStruct((n_ep, CAP, width), BF),
            jax.ShapeDtypeStruct((nz, nx, 2, positions, 2 * vdim), BF),
            jax.ShapeDtypeStruct((n_tp, width, hid), BF),
            jax.ShapeDtypeStruct((n_tp, width, hid), BF),
            jax.ShapeDtypeStruct((n_tp, hid, width), BF),
        ],
        in_specs=[ANY] * 5,
        out_specs=[ANY] * 5,
        scratch_shapes=[
            pltpu.VMEM((CAP, width), BF),
            pltpu.VMEM((positions, 2 * vdim), BF),
            pltpu.VMEM((width, hid), BF),
            pltpu.VMEM((hid, width), BF),
            sem((2, 3)), sem((2, 3)), sem((2, 3)), sem((2, 3)),
            sem((nz,)), sem((nz,)), sem((2,)), sem((2,)), sem((2,)), sem((2,)),
            sem((4,)), sem((4,)), sem((n_ep,)), sem((n_ep,)), sem((4,)),
        ],
        compiler_params=pltpu.CompilerParams(
            collective_id=0, has_side_effects=True, vmem_limit_bytes=8 * 1024 * 1024
        ),
        name="exchange",
    )(outgoing.reshape(n_ep, CAP, width), kv, w_gate[0], w_up[0], w_down[0])

    expert_out = pl.pallas_call(
        expert_kernel,
        grid=(n_tp,),
        out_shape=jax.ShapeDtypeStruct((slots, width), BF),
        in_specs=[
            pl.BlockSpec((slots, width), lambda g: (0, 0)),
            pl.BlockSpec((1, width, hid), lambda g: (g, 0, 0)),
            pl.BlockSpec((1, width, hid), lambda g: (g, 0, 0)),
            pl.BlockSpec((1, hid, width), lambda g: (g, 0, 0)),
        ],
        out_specs=pl.BlockSpec((slots, width), lambda g: (0, 0)),
        scratch_shapes=[pltpu.VMEM((slots, width), F32)],
        compiler_params=params(),
        cost_estimate=pl.CostEstimate(
            flops=6 * slots * width * hid * n_tp, bytes_accessed=16 * 1024 * 1024, transcendentals=0
        ),
        name="expert",
    )(arrived.reshape(slots, width), g_all, u_all, d_all)

    back = lax.all_to_all(
        expert_out.reshape(1, n_ep, CAP, width), "ep", split_axis=1, concat_axis=1, tiled=True
    )[0].reshape(slots, width)

    blk = 1024
    length = n_ep * positions
    attn_rows = pl.pallas_call(
        functools.partial(attention_kernel, blk),
        out_shape=jax.ShapeDtypeStruct((positions, heads * vdim), BF),
        in_specs=[VM, VM, pl.BlockSpec(memory_space=pltpu.SMEM), VM],
        out_specs=VM,
        scratch_shapes=[
            pltpu.VMEM((2 * heads, positions, vdim), BF),
            pltpu.VMEM((2 * heads, positions, 128), F32),
            pltpu.VMEM((2 * heads, positions, 2 * vdim), F32),
        ],
        compiler_params=params(),
        cost_estimate=pl.CostEstimate(
            flops=2 * 2 * heads * positions * length * 3 * vdim,
            bytes_accessed=length * 4 * vdim,
            transcendentals=2 * heads * positions * length,
        ),
        name="attend",
    )(
        jnp.transpose(queries, (1, 0, 2)),
        kv_all.reshape(length, 2 * vdim),
        attn_lambda,
        head_gain.reshape(1, vdim),
    )
    tiles = lax.all_to_all(
        attn_rows.reshape(n_tp, positions // n_tp, heads * vdim), "tp", 0, 0, tiled=True
    )
    mixer_out = jnp.einsum(
        "gsk,gkd->sd", tiles, w_out.reshape(n_tp, heads * vdim, width), preferred_element_type=F32
    ).astype(BF)

    moe_out = pl.pallas_call(
        combine_kernel,
        out_shape=jax.ShapeDtypeStruct((dev_rows, width), BF),
        in_specs=[VM, VM, VM],
        out_specs=VM,
        compiler_params=params(),
        name="combine",
    )(back, own_routes, own_weights)
    return (mixer_out, moe_out)


def solution(mesh):
    return jax.shard_map(
        local,
        mesh=mesh,
        in_specs=(
            P("ep", "tp", None),
            P("ep", "tp", None),
            P("ep", "tp", None),
            P("tp"),
            P(),
            P(),
            P("ep", None),
            P(),
            P("ep", None),
            P("ep", None),
            P("ep", None, "tp"),
            P("ep", None, "tp"),
            P("ep", "tp", None),
        ),
        out_specs=(P(("ep", "tp"), None), P(("ep", "tp"), None)),
        check_vma=False,
    )
```

time: 438 us -> 243 us (0.55)
  Pallas kernels: 0 us -> 139 us
  waiting for transfers between devices: 181 us -> 44.5 us
  local copies, waits for them, and re-layouts: 98.3 us -> 16.2 us
  blocking collectives: 71.2 us -> 0 us
  matrix products: 26.3 us -> 3.73 us
  starting transfers between devices: 18.4 us -> 35.3 us
  between operations: 14.1 us -> 0.77 us
  other arithmetic: 13.3 us -> 0.89 us
  loops' own time: 9.78 us -> 0 us
    pallas_call x0 -> x5, Pallas kernels: none -> 139 us  [the longest x1 115 us: local(): pl.pallas_call(functools.partial(comm_kernel, n_ep, n_tp, nz, nx), out_sh...]
    all_gather x4 -> x0, waiting for transfers between devices: 116 us -> none  [the longest x1 50.1 us: piecewise(): tiles = [lax.all_gather(section, axis) for section in pieces]]
    all_to_all x1 -> x0, blocking collectives: 71.2 us -> none  [local(): lax.all_to_all(outgoing, 'ep', split_axis=0, concat_axis=0, tiled=True)]
    scatter x1 -> x0, local copies, waits for them, and re-layouts: 33 us -> none  [fill_slots(): return (blank_slots.at[block_routes, slot_ids].set(copies), slot_ids)]
    dot_general x11 -> x1, matrix products: 26.3 us -> 3.73 us  [local(): jnp.einsum('gsk,gkd->sd', tiles, w_out.reshape(n_tp, heads * vdim, width)...]
    all_to_all x3 -> x2, waiting for transfers between devices: 64.1 us -> 44.5 us  [the longest x1 44.5 us: local(): lax.all_to_all(expert_out.reshape(1, n_ep, CAP, width), 'ep', split_axis=...]
    all_to_all x3 -> x2, starting transfers between devices: 18.1 us -> 35.3 us  [the longest x1 32 us: local(): lax.all_to_all(expert_out.reshape(1, n_ep, CAP, width), 'ep', split_axis=...]
    reshape x2 -> x0, local copies, waits for them, and re-layouts: 14.8 us -> none  [the longest x1 14.7 us: local(): key_blocks = key_piece.reshape(blocks, block_len, kv_heads, 2, head_dim)]
  transfers between devices with their start and end apart: 7 -> 2, of which waited for: 5 -> 1; matrix products, arithmetic and copies ran while one was open for 29% -> 2% of each run, Pallas kernels for 0% -> 4%
where the time goes in v1:
time: 243 us; the launch traced here: 240 us
  Pallas kernels  139 us (57%)
  waiting for transfers between devices  44.5 us (18%)
  starting transfers between devices  35.3 us (15%)
  local copies, waits for them, and re-layouts  16.2 us (7%)
  matrix products  3.73 us (2%)
    pallas_call x1, Pallas kernels, local(): pl.pallas_call(functools.partial(comm_kernel, n_ep, n_tp, nz, nx), out_sh...  115 us
    all_to_all x1, waiting for transfers between devices, local(): lax.all_to_all(expert_out.reshape(1, n_ep, CAP, width), 'ep', split_axis=...  44.5 us
    all_to_all x1, starting transfers between devices, local(): lax.all_to_all(expert_out.reshape(1, n_ep, CAP, width), 'ep', split_axis=...  32 us
    unnamed x31, local copies, waits for them, and re-layouts  14.6 us
    pallas_call x1, Pallas kernels, local(): pl.pallas_call(expert_kernel, grid=(n_tp,), out_shape=jax.ShapeDtypeStruc...  10.5 us
    pallas_call x1, Pallas kernels, local(): pl.pallas_call(functools.partial(attention_kernel, blk), out_shape=jax.Sh...  8.91 us
  transfers between devices with their start and end apart: 2, of which 1 were waited for; matrix products, arithmetic and copies ran while one was open for 2% of the time, Pallas kernels for 4%

profile of v1, /device:TPU:7, one launch (start us, length us, event | category | flops | bytes accessed | tf_op | source)
XLA Modules:
  0.0 240.3 jit_solution(16008129625415095527)
XLA Ops:
  0.6 0.0 copy-start
  0.6 0.0 copy-start.2
  0.7 0.8 constant_dynamic-slice_fusion.1
  1.5 0.1 copy.24.routes_ref
  1.6 0.1 copy.21.routes_ref
  1.7 0.6 copy-done
  2.2 0.0 copy-start.3
  2.2 0.0 copy-start.4
  2.3 1.1 copy.27
  3.4 0.9 pad_maximum_fusion.kv_ref
  4.2 0.0 copy-start.5
  4.3 0.7 copy-done.5
  5.0 0.0 copy-start.12
  5.0 0.0 copy-start.13
  5.0 0.9 pack.1
  5.9 0.0 copy-done.2
  5.9 0.0 copy-done.3
  5.9 0.0 copy-done.4
  5.9 115.3 %exchange.1 = (bf16[64,8,2048]{2,1,0:T(8,128)(2,1)S(1)}, bf16[8,4,2,256,256]{4,3,2,1,0:T(8,128)(2,1)S(1)}, bf16[4,2048,256]{2,1,0:T(8,128)(2,1)S(1)}, bf16[4,204...) custom-call(bf16[64,8,2048]{2,1,0:T(8,128)(2,1)S(1)} %bitcast.26, bf16[256,256]{1,0:T(8,128)(2,1)S(1)} %pad_maximum_fusion.kv_ref, ...), custom_call_target="tpu_custom_call" | custom-call | tf_op jit(solution)/shard_map/exchange/pallas_call | solution.py:350
  121.2 0.0 copy-start.6
  121.2 3.2 %copy-done.6 = bf16[8,4,2,256,256]{4,3,2,1,0:T(8,128)(2,1)} copy-done((bf16[8,4,2,256,256]{4,3,2,1,0:T(8,128)(2,1)}, bf16[8,4,2,256,256]{4,3,2,1,0:T(8,128)(2,1)S(1)}, u32[]{:S(2)}) %copy-start.6) | copy-done | bytes 8388632
  124.5 0.0 copy-start.7
  124.5 2.0 copy-done.7
  126.4 0.0 copy-start.8
  126.4 1.9 copy-done.8
  128.4 0.0 copy-start.9
  128.4 1.9 copy-done.9
  130.3 0.0 copy-start.10
  130.3 0.0 copy-done.12
  130.3 0.0 copy-done.13
  130.3 8.9 %attend.1 = bf16[256,256]{1,0:T(8,128)(2,1)} custom-call(bf16[2,256,128]{2,1,0:T(8,128)(2,1)S(1)} %bitcast.32, bf16[16384,256]{1,0:T(8,128)(2,1)} %bitcast.34, f32[2]{0:T(128)S(1)} %copy-done.12, f32[1,128]{1,0:T(1,128)S(1)} %bitcast.36), custom_call_target="tpu_custom_call" | custom-call | flops 12884901888 | bytes 8388608 | tf_op jit(solution)/shard_map/attend/pallas_call | solution.py:401
  139.2 0.0 copy-done.10
  139.2 3.3 %all-to-all-start = ((bf16[4,64,256]{2,1,0:T(8,128)(2,1)}), bf16[4,64,256]{2,1,0:T(8,128)(2,1)S(1)}, u32[]{:S(2)}, u32[]{:S(2)}) async-start(bf16[4,64,256]{2,1,0:T(8,128)(2,1)} %bitcast.11), calls=%async_computation | async-start | bytes 262144 | tf_op jit(solution)/shard_map/all_to_all | solution.py:424
  142.6 0.0 copy-start.11
  142.6 1.6 copy-done.11
  144.2 10.5 %expert.1 = bf16[512,2048]{1,0:T(8,128)(2,1)S(1)} custom-call(bf16[512,2048]{1,0:T(8,128)(2,1)S(1)} %bitcast.35, bf16[4,2048,256]{2,1,0:T(8,128)(2,1)} %copy-done.7, bf16[4,2048,256]{2,1,0:T(8,128)(2,1)} %copy-done.8, bf16[4,256,2048]{2,1,0:T(8,128)(2,1)} %copy-done.9), custom_call_target="tpu_custom_call" | custom-call | flops 6442450944 | bytes 16777216 | tf_op jit(solution)/shard_map/expert/pallas_call | solution.py:376
  154.7 0.0 copy-start.1
  154.7 1.3 copy-done.1
  156.0 0.0 all-to-all-done
  156.0 32.0 %all-to-all-start.1 = ((bf16[1,64,8,2048]{3,2,0,1:T(8,128)(2,1)}), bf16[1,64,8,2048]{3,2,0,1:T(8,128)(2,1)}, u32[]{:S(2)}, u32[]{:S(2)}) async-start(bf16[1,64,8,2048]{3,2,0,1:T(8,128)(2,1)} %bitcast.27), calls=%async_computation.1 | async-start | bytes 4194304 | tf_op jit(solution)/shard_map/all_to_all | solution.py:395
  188.0 0.7 constant_dynamic-slice_fusion
  188.6 0.1 copy.25.weights_ref
  188.8 3.7 %fusion = bf16[64,2048]{1,0:T(8,128)(2,1)} fusion(bf16[4,64,256]{2,1,0:T(8,128)(2,1)S(1)} %all-to-all-done, bf16[4,256,2048]{2,1,0:T(8,128)(2,1)} %bitcast.37), kind=kOutput, calls=%fused_computation.1 | convolution fusion | flops 268566528 | bytes 4587520 | tf_op jit(solution)/shard_map/gsk,gkd->sd/dot_general | solution.py:427
  192.5 44.5 %all-to-all-done.1 = bf16[1,64,8,2048]{3,2,0,1:T(8,128)(2,1)} async-done(((bf16[1,64,8,2048]{3,2,0,1:T(8,128)(2,1)}), bf16[1,64,8,2048]{3,2,0,1:T(8,128)(2,1)}, u32[]{:S(2)}, u32[]{:S(2)}) %all-to-all-start.1) | async-done | bytes 2097184 | tf_op jit(solution)/shard_map/all_to_all | solution.py:395
  237.0 3.4 %combine.1 = bf16[128,2048]{1,0:T(8,128)(2,1)} custom-call(bf16[512,2048]{1,0:T(8,128)(2,1)} %bitcast.17.back_ref, s32[128,2]{1,0:T(8,128)S(1)} %copy.24.routes_ref, f32[128,2]{1,0:T(8,128)S(1)} %copy.25.weights_ref), custom_call_target="tpu_custom_call" | custom-call | tf_op jit(solution)/shard_map/combine/pallas_call | solution.py:431
  (1 shorter events, 0.0 us)
Async XLA Ops:
  0.6 1.6 copy-start
  0.6 5.3 %copy-start.2 = (bf16[1,2048,256]{2,1,0:T(8,128)(2,1)S(1)}, bf16[1,2048,256]{2,1,0:T(8,128)(2,1)}, u32[]{:S(2)}) copy-start(bf16[1,2048,256]{2,1,0:T(8,128)(2,1)} %param.23) | copy-start | bytes 3145732
  2.2 3.7 %copy-start.3 = (bf16[1,2048,256]{2,1,0:T(8,128)(2,1)S(1)}, bf16[1,2048,256]{2,1,0:T(8,128)(2,1)}, u32[]{:S(2)}) copy-start(bf16[1,2048,256]{2,1,0:T(8,128)(2,1)} %param.24) | copy-start | bytes 3145732
  2.2 3.7 %copy-start.4 = (bf16[1,256,2048]{2,1,0:T(8,128)(2,1)S(1)}, bf16[1,256,2048]{2,1,0:T(8,128)(2,1)}, u32[]{:S(2)}) copy-start(bf16[1,256,2048]{2,1,0:T(8,128)(2,1)} %param.25) | copy-start | bytes 3145732
  4.2 0.7 copy-start.5
  5.0 125.4 %copy-start.12 = (f32[2]{0:T(128)S(1)}, f32[2]{0:T(128)}, u32[]{:S(2)}) copy-start(f32[2]{0:T(128)} %lam_ref.1) | copy-start | bytes 28
  5.0 125.4 %copy-start.13 = (f32[128]{0:T(128)S(1)}, f32[128]{0:T(128)}, u32[]{:S(2)}) copy-start(f32[128]{0:T(128)} %param.17) | copy-start | bytes 1540
  121.2 3.2 %copy-start.6 = (bf16[8,4,2,256,256]{4,3,2,1,0:T(8,128)(2,1)}, bf16[8,4,2,256,256]{4,3,2,1,0:T(8,128)(2,1)S(1)}, u32[]{:S(2)}) copy-start(bf16[8,4,2,256,256]{4,3,2,1,0:T(8,128)(2,1)S(1)} %get-tuple-element.7) | copy-start | bytes 25165828
  124.5 2.0 copy-start.7
  126.4 1.9 copy-start.8
  128.4 2.0 copy-start.9
  130.3 8.9 %copy-start.10 = (bf16[64,8,2048]{2,1,0:T(8,128)(2,1)}, bf16[64,8,2048]{2,1,0:T(8,128)(2,1)S(1)}, u32[]{:S(2)}) copy-start(bf16[64,8,2048]{2,1,0:T(8,128)(2,1)S(1)} %get-tuple-element.8) | copy-start | bytes 6291460
  139.2 16.8 %all-to-all-start = ((bf16[4,64,256]{2,1,0:T(8,128)(2,1)}), bf16[4,64,256]{2,1,0:T(8,128)(2,1)S(1)}, u32[]{:S(2)}, u32[]{:S(2)}) async-start(bf16[4,64,256]{2,1,0:T(8,128)(2,1)} %bitcast.11), calls=%async_computation | async-start | bytes 262144 | tf_op jit(solution)/shard_map/all_to_all | solution.py:424
  142.6 1.6 copy-start.11
  154.7 1.3 copy-start.1
  156.0 81.0 %all-to-all-start.1 = ((bf16[1,64,8,2048]{3,2,0,1:T(8,128)(2,1)}), bf16[1,64,8,2048]{3,2,0,1:T(8,128)(2,1)}, u32[]{:S(2)}, u32[]{:S(2)}) async-start(bf16[1,64,8,2048]{3,2,0,1:T(8,128)(2,1)} %bitcast.27), calls=%async_computation.1 | async-start | bytes 4194304 | tf_op jit(solution)/shard_map/all_to_all | solution.py:395

commit v2 on v1

--- a/solution.py
+++ b/solution.py
@@ -84,9 +84,9 @@
 
 def comm_kernel(
     n_ep, n_tp, nz, nx,
-    slots_ref, kv_ref, wg_ref, wu_ref, wd_ref,
-    arrived_ref, kv_all_ref, g_ref, u_ref, d_ref,
-    slot_tmp, kv_tmp, w_tmp, wd_tmp,
+    slots_ref, kv_ref, wg_ref, wu_ref, wd_ref, q_ref, lam_ref, gain_ref,
+    arrived_ref, g_ref, u_ref, d_ref, attn_ref,
+    kv_all_ref, slot_tmp, w_tmp, wd_tmp, q_s, m_s, acc_s,
     w_send, w_recv, f_send, f_recv, z_send, z_recv, x_send, x_recv, y_send, y_recv,
     c_send, c_recv, d_send, d_recv, local_sem,
 ):
@@ -157,7 +157,9 @@
         push.start()
         push.wait()
 
-    stay(kv_ref, kv_tmp, kv_all_ref.at[z, x, c], 0)
+    own_kv = pltpu.make_async_copy(kv_ref, kv_all_ref.at[z, x, c], local_sem.at[0])
+    own_kv.start()
+    own_kv.wait()
     stay(slots_ref.at[me], slot_tmp, arrived_ref.at[me], 1)
     stay(wg_ref, w_tmp, g_ref.at[tp], 2)
     stay(wu_ref, w_tmp, u_ref.at[tp], 2)
@@ -224,14 +226,23 @@
     on_right.wait_recv()
     on_left.wait_recv()
     across(3, x2).start()
+    for n, xx in enumerate((x, xl, xr, x2)):
+        across(n, xx).wait()
+    n_pos = kv_ref.shape[0]
+
+    def kv_block(b):
+        pieces = [
+            kv_all_ref[b // (nx // 2), 2 * lax.rem(b, nx // 2) + j // 2, j % 2] for j in range(4)
+        ]
+        return jnp.concatenate(pieces, axis=0)
+
+    attend(me, 4 * n_pos, q_ref, kv_block, lam_ref, gain_ref, attn_ref, q_s, m_s, acc_s)
 
     def row_wait(d, carry):
         row_copy(d).wait()
         return carry
 
     lax.fori_loop(1, n_ep, row_wait, 0)
-    for n, xx in enumerate((x, xl, xr, x2)):
-        across(n, xx).wait()
     for w in weights:
         w.wait_send()
     for i in range(3):
@@ -263,8 +274,7 @@
         out_ref[...] = acc_ref[...].astype(BF)
 
 
-def attention_kernel(blk, q_ref, kv_ref, lam_ref, gain_ref, out_ref, q_s, m_s, acc_s):
-    me = lax.axis_index("ep")
+def attend(me, blk, q_ref, kv_block, lam_ref, gain_ref, out_ref, q_s, m_s, acc_s):
     rows = q_ref.shape[1]
     heads = q_ref.shape[0]
     vdim = q_ref.shape[2]
@@ -279,8 +289,8 @@
 
     def block(b, masked):
         start = pl.multiple_of(b * blk, blk)
-        k = kv_ref[pl.ds(start, blk), 0:vdim]
-        v = kv_ref[pl.ds(start, blk), vdim : 2 * vdim]
+        kv = kv_block(b)
+        k, v = kv[:, 0:vdim], kv[:, vdim : 2 * vdim]
         v_one = jnp.concatenate([v, jnp.ones_like(v)], axis=1)
         for r in range(2 * heads):
             s = lax.dot_general(
@@ -347,31 +357,37 @@
 
     kv = jnp.concatenate([keys[:, 0], values[:, 0]], axis=1)
     sem = pltpu.SemaphoreType.DMA
-    arrived, kv_all, g_all, u_all, d_all = pl.pallas_call(
+    arrived, g_all, u_all, d_all, attn_rows = pl.pallas_call(
         functools.partial(comm_kernel, n_ep, n_tp, nz, nx),
         out_shape=[
             jax.ShapeDtypeStruct((n_ep, CAP, width), BF),
-            jax.ShapeDtypeStruct((nz, nx, 2, positions, 2 * vdim), BF),
             jax.ShapeDtypeStruct((n_tp, width, hid), BF),
             jax.ShapeDtypeStruct((n_tp, width, hid), BF),
             jax.ShapeDtypeStruct((n_tp, hid, width), BF),
+            jax.ShapeDtypeStruct((positions, heads * vdim), BF),
         ],
-        in_specs=[ANY] * 5,
-        out_specs=[ANY] * 5,
+        in_specs=[ANY] * 5 + [VM, pl.BlockSpec(memory_space=pltpu.SMEM), VM],
+        out_specs=[ANY] * 4 + [VM],
         scratch_shapes=[
+            pltpu.VMEM((nz, nx, 2, positions, 2 * vdim), BF),
             pltpu.VMEM((CAP, width), BF),
-            pltpu.VMEM((positions, 2 * vdim), BF),
             pltpu.VMEM((width, hid), BF),
             pltpu.VMEM((hid, width), BF),
+            pltpu.VMEM((2 * heads, positions, vdim), BF),
+            pltpu.VMEM((2 * heads, positions, 128), F32),
+            pltpu.VMEM((2 * heads, positions, 2 * vdim), F32),
             sem((2, 3)), sem((2, 3)), sem((2, 3)), sem((2, 3)),
             sem((nz,)), sem((nz,)), sem((2,)), sem((2,)), sem((2,)), sem((2,)),
             sem((4,)), sem((4,)), sem((n_ep,)), sem((n_ep,)), sem((4,)),
         ],
         compiler_params=pltpu.CompilerParams(
-            collective_id=0, has_side_effects=True, vmem_limit_bytes=8 * 1024 * 1024
+            collective_id=0, has_side_effects=True, vmem_limit_bytes=56 * 1024 * 1024
         ),
         name="exchange",
-    )(outgoing.reshape(n_ep, CAP, width), kv, w_gate[0], w_up[0], w_down[0])
+    )(
+        outgoing.reshape(n_ep, CAP, width), kv, w_gate[0], w_up[0], w_down[0],
+        jnp.transpose(queries, (1, 0, 2)), attn_lambda, head_gain.reshape(1, vdim),
+    )
 
     expert_out = pl.pallas_call(
         expert_kernel,
@@ -396,31 +412,6 @@
         expert_out.reshape(1, n_ep, CAP, width), "ep", split_axis=1, concat_axis=1, tiled=True
     )[0].reshape(slots, width)
 
-    blk = 1024
-    length = n_ep * positions
-    attn_rows = pl.pallas_call(
-        functools.partial(attention_kernel, blk),
-        out_shape=jax.ShapeDtypeStruct((positions, heads * vdim), BF),
-        in_specs=[VM, VM, pl.BlockSpec(memory_space=pltpu.SMEM), VM],
-        out_specs=VM,
-        scratch_shapes=[
-            pltpu.VMEM((2 * heads, positions, vdim), BF),
-            pltpu.VMEM((2 * heads, positions, 128), F32),
-            pltpu.VMEM((2 * heads, positions, 2 * vdim), F32),
-        ],
-        compiler_params=params(),
-        cost_estimate=pl.CostEstimate(
-            flops=2 * 2 * heads * positions * length * 3 * vdim,
-            bytes_accessed=length * 4 * vdim,
-            transcendentals=2 * heads * positions * length,
-        ),
-        name="attend",
-    )(
-        jnp.transpose(queries, (1, 0, 2)),
-        kv_all.reshape(length, 2 * vdim),
-        attn_lambda,
-        head_gain.reshape(1, vdim),
-    )
     tiles = lax.all_to_all(
         attn_rows.reshape(n_tp, positions // n_tp, heads * vdim), "tp", 0, 0, tiled=True
     )

time: 243 us -> 217 us (0.89)
  starting transfers between devices: 35.3 us -> 22.2 us
  local copies, waits for them, and re-layouts: 16.2 us -> 8.96 us
  Pallas kernels: 139 us -> 132 us
    all_to_all x1, starting transfers between devices: 32 us -> 18.9 us  [local(): lax.all_to_all(expert_out.reshape(1, n_ep, CAP, width), 'ep', split_axis=...]
    pallas_call x1 -> x0, Pallas kernels: 8.91 us -> none  [local(): pl.pallas_call(functools.partial(attention_kernel, blk), out_shape=jax.Sh...]
    unnamed x31 -> x13, local copies, waits for them, and re-layouts: 14.6 us -> 7.34 us
  transfers between devices with their start and end apart: 2 -> 2, of which waited for: 1 -> 1; matrix products, arithmetic and copies ran while one was open for 2% -> 2% of each run, Pallas kernels for 4% -> 5%
where the time goes in v2:
time: 217 us; the launch traced here: 213 us
  Pallas kernels  132 us (61%)
  waiting for transfers between devices  44.5 us (21%)
  starting transfers between devices  22.2 us (10%)
  local copies, waits for them, and re-layouts  8.96 us (4%)
  matrix products  3.73 us (2%)
    pallas_call x1, Pallas kernels, local(): pl.pallas_call(functools.partial(comm_kernel, n_ep, n_tp, nz, nx), out_sh...  117 us
    all_to_all x1, waiting for transfers between devices, local(): lax.all_to_all(expert_out.reshape(1, n_ep, CAP, width), 'ep', split_axis=...  44.5 us
    all_to_all x1, starting transfers between devices, local(): lax.all_to_all(expert_out.reshape(1, n_ep, CAP, width), 'ep', split_axis=...  18.9 us
    pallas_call x1, Pallas kernels, local(): pl.pallas_call(expert_kernel, grid=(n_tp,), out_shape=jax.ShapeDtypeStruc...  10.5 us
    unnamed x13, local copies, waits for them, and re-layouts  7.34 us
  transfers between devices with their start and end apart: 2, of which 1 were waited for; matrix products, arithmetic and copies ran while one was open for 2% of the time, Pallas kernels for 5%

profile of v2, /device:TPU:7, one launch (start us, length us, event | category | flops | bytes accessed | tf_op | source)
XLA Modules:
  0.0 213.5 jit_solution(4380275239535160445)
XLA Ops:
  0.6 0.0 copy-start
  0.6 0.8 constant_dynamic-slice_fusion.1
  1.5 0.1 copy.24.routes_ref
  1.6 0.1 copy.20.routes_ref
  1.7 0.6 copy-done
  2.3 1.6 copy.27
  3.9 1.5 pad_maximum_fusion.kv_ref
  5.4 0.0 copy-start.3
  5.4 0.7 copy-done.3
  6.1 0.9 pack.1
  7.0 0.0 copy-start.1
  7.1 1.3 copy-done.1
  8.4 117.0 %exchange.1 = (bf16[64,8,2048]{2,1,0:T(8,128)(2,1)}, bf16[4,2048,256]{2,1,0:T(8,128)(2,1)}, bf16[4,2048,256]{2,1,0:T(8,128)(2,1)}, bf16[4,256,2048]{2,1,0:T(8,128)(2,1)}, bf16[256,256]{1,0:T(8,128)(2,1)}) custom-call(bf16[64,8,2048]{2,1,0:T(8,128)(2,1)} %bitcast.25, bf16[256,256]{1,0:T(8,128)(2,1)} %pad_maximum_fusion.kv_ref, bf16[2048,256]{1,0:T(8,128)(2,1)} %bitcast.31, ...), custom_call_target="tpu_custom_call" | custom-call | tf_op jit(solution)/shard_map/exchange/pallas_call | solution.py:360
  125.4 3.3 %all-to-all-start = ((bf16[4,64,256]{2,1,0:T(8,128)(2,1)}), bf16[4,64,256]{2,1,0:T(8,128)(2,1)S(1)}, u32[]{:S(2)}, u32[]{:S(2)}) async-start(bf16[4,64,256]{2,1,0:T(8,128)(2,1)} %bitcast.35), calls=%async_computation | async-start | bytes 262144 | tf_op jit(solution)/shard_map/all_to_all | solution.py:415
  128.7 0.0 copy-start.4
  128.8 1.6 copy-done.4
  130.3 10.5 %expert.1 = bf16[512,2048]{1,0:T(8,128)(2,1)S(1)} custom-call(bf16[512,2048]{1,0:T(8,128)(2,1)S(1)} %bitcast.29, bf16[4,2048,256]{2,1,0:T(8,128)(2,1)} %get-tuple-element.9.g_ref, bf16[4,2048,256]{2,1,0:T(8,128)(2,1)} %get-tuple-element.10.u_ref, bf16[4,256,2048]{2,1,0:T(8,128)(2,1)} %get-tuple-element.11.d_ref), custom_call_target="tpu_custom_call" | custom-call | flops 6442450944 | bytes 16777216 | tf_op jit(solution)/shard_map/expert/pallas_call | solution.py:392
  140.9 0.0 copy-start.2
  140.9 1.3 copy-done.2
  142.2 0.0 all-to-all-done
  142.2 18.9 %all-to-all-start.1 = ((bf16[1,64,8,2048]{3,2,0,1:T(8,128)(2,1)}), bf16[1,64,8,2048]{3,2,0,1:T(8,128)(2,1)}, u32[]{:S(2)}, u32[]{:S(2)}) async-start(bf16[1,64,8,2048]{3,2,0,1:T(8,128)(2,1)} %bitcast.26), calls=%async_computation.1 | async-start | bytes 4194304 | tf_op jit(solution)/shard_map/all_to_all | solution.py:411
  161.1 0.7 constant_dynamic-slice_fusion
  161.8 0.1 copy.25.weights_ref
  161.9 3.7 %fusion = bf16[64,2048]{1,0:T(8,128)(2,1)} fusion(bf16[4,64,256]{2,1,0:T(8,128)(2,1)S(1)} %all-to-all-done, bf16[4,256,2048]{2,1,0:T(8,128)(2,1)} %bitcast.30), kind=kOutput, calls=%fused_computation.1 | convolution fusion | flops 268566528 | bytes 4587520 | tf_op jit(solution)/shard_map/gsk,gkd->sd/dot_general | solution.py:418
  165.6 44.5 %all-to-all-done.1 = bf16[1,64,8,2048]{3,2,0,1:T(8,128)(2,1)} async-done(((bf16[1,64,8,2048]{3,2,0,1:T(8,128)(2,1)}), bf16[1,64,8,2048]{3,2,0,1:T(8,128)(2,1)}, u32[]{:S(2)}, u32[]{:S(2)}) %all-to-all-start.1) | async-done | bytes 2097184 | tf_op jit(solution)/shard_map/all_to_all | solution.py:411
  210.1 3.4 %combine.1 = bf16[128,2048]{1,0:T(8,128)(2,1)} custom-call(bf16[512,2048]{1,0:T(8,128)(2,1)} %bitcast.16.back_ref, s32[128,2]{1,0:T(8,128)S(1)} %copy.24.routes_ref, f32[128,2]{1,0:T(8,128)S(1)} %copy.25.weights_ref), custom_call_target="tpu_custom_call" | custom-call | tf_op jit(solution)/shard_map/combine/pallas_call | solution.py:422
  (1 shorter events, 0.0 us)
Async XLA Ops:
  0.6 1.6 copy-start
  5.4 0.7 copy-start.3
  7.0 1.3 copy-start.1
  125.4 16.8 %all-to-all-start = ((bf16[4,64,256]{2,1,0:T(8,128)(2,1)}), bf16[4,64,256]{2,1,0:T(8,128)(2,1)S(1)}, u32[]{:S(2)}, u32[]{:S(2)}) async-start(bf16[4,64,256]{2,1,0:T(8,128)(2,1)} %bitcast.35), calls=%async_computation | async-start | bytes 262144 | tf_op jit(solution)/shard_map/all_to_all | solution.py:415
  128.7 1.6 copy-start.4
  140.9 1.3 copy-start.2
  142.2 67.9 %all-to-all-start.1 = ((bf16[1,64,8,2048]{3,2,0,1:T(8,128)(2,1)}), bf16[1,64,8,2048]{3,2,0,1:T(8,128)(2,1)}, u32[]{:S(2)}, u32[]{:S(2)}) async-start(bf16[1,64,8,2048]{3,2,0,1:T(8,128)(2,1)} %bitcast.26), calls=%async_computation.1 | async-start | bytes 4194304 | tf_op jit(solution)/shard_map/all_to_all | solution.py:411
